TPU v7x, 32 devices: a whole 2x2x4 slice. The times are simulated.
32 devices in a mesh: sp: 4 (over z), fs: 4 (over y, core), tp: 2 (over x).
Axes of the slice: x: 2, y: 2, z: 4, core: 2. Of those that a mesh axis runs over, the one named last changes fastest.
Arguments:
- tokens: bfloat16 [4, 4096, 2048], P('fs', 'sp', 'tp'), may hold values from -8 to 8
- norm_gain: float32 [2048], replicated, may hold values from 0.1 to 1.9
- w_query: bfloat16 [2048, 1024], P(('sp', 'fs'), 'tp'), may hold values from -4 to 4
- w_key: bfloat16 [2048, 512], P(('sp', 'fs'), 'tp'), may hold values from -0.16 to 0.16
- w_value: bfloat16 [2048, 512], P(('sp', 'fs'), 'tp'), may hold values from -0.125 to 0.125
- w_conv_in: bfloat16 [2048, 1024], P(('sp', 'fs'), 'tp'), may hold values from -0.125 to 0.125
- w_conv_b: bfloat16 [2048, 1024], P(('sp', 'fs'), 'tp'), may hold values from -0.125 to 0.125
- w_conv_c: bfloat16 [2048, 1024], P(('sp', 'fs'), 'tp'), may hold values from -0.125 to 0.125
- conv_taps: bfloat16 [3, 1024], P(None, 'tp'), may hold values from -3.5 to 3.5
- sink_logits: float32 [16], P('tp'), may hold values from 1 to 5
- w_attn_out: bfloat16 [1024, 2048], P('tp', ('sp', 'fs')), may hold values from -0.375 to 0.375
- w_conv_out: bfloat16 [1024, 2048], P('tp', ('sp', 'fs')), may hold values from -0.125 to 0.125
Outputs:
- mixed: bfloat16 [4, 4096, 2048], P('fs', ('sp', 'tp'))
All inputs are finite; a program needn't handle non-finite values.
Results may differ from a plain program's by a relative error of at most 0.02.
Values may be sent and summed in bfloat16 or wider, within the bound.
A program may use at most 128 MiB of HBM per device.

v0:
```python
import jax
import jax.numpy as jnp
from jax import lax
from jax.sharding import PartitionSpec as P

HEADS = 16
HEAD = 64
WINDOW = 128


def shifted(block, axis, distance):
    devices = range(lax.axis_size(axis))
    route = [(i - distance, i) for i in devices if i - distance in devices]
    return lax.ppermute(block, axis, route)


def norm_rows(tokens, norm_gain):
    values = tokens.astype(jnp.float32)
    average = jnp.mean(values, axis=-1, keepdims=True)
    centred = values - average
    variance = jnp.mean(centred * centred, axis=-1, keepdims=True)
    return (centred * lax.rsqrt(variance + 1e-05) * norm_gain).astype(jnp.bfloat16)


def attend(queries, keys_values, earlier_rows, sink_logits, head_base, row_base):
    row_total = queries.shape[0]
    kv_cols = keys_values.shape[1] // 2
    kv_here = kv_cols // HEAD
    heads_here = queries.shape[1] // HEAD
    group = heads_here // kv_here
    keys_all = jnp.concatenate([earlier_rows, keys_values], axis=0)
    block_rows = min(512, row_total)
    head_ids = head_base + jnp.arange(heads_here, dtype=jnp.int32)
    slopes = jnp.exp2(-8.0 * (head_ids + 1).astype(jnp.float32) / HEADS).reshape(kv_here, group)[
        :, :, None, None
    ]
    sinks = sink_logits.reshape(kv_here, group)[:, :, None, None]
    row_ids = jnp.arange(block_rows, dtype=jnp.int32)[:, None]
    col_ids = jnp.arange(block_rows + WINDOW, dtype=jnp.int32)[None, :]
    distance = WINDOW + row_ids - col_ids
    outputs = []
    for block in range(row_total // block_rows):
        first_row = block * block_rows
        query_block = queries[first_row : first_row + block_rows].reshape(
            block_rows, kv_here, group, HEAD
        )
        band = keys_all[first_row : first_row + block_rows + WINDOW]
        band_keys = band[:, :kv_cols].reshape(block_rows + WINDOW, kv_here, HEAD)
        band_values = band[:, kv_cols:].reshape(block_rows + WINDOW, kv_here, HEAD)
        scores = jnp.einsum(
            "qkgd,skd->kgqs", query_block, band_keys, preferred_element_type=jnp.float32
        ) * HEAD ** (-0.5)
        scores = scores - slopes * distance.astype(jnp.float32)
        key_place = row_base + first_row - WINDOW + col_ids
        keep = (distance >= 0) & (distance < WINDOW) & (key_place >= 0)
        scores = jnp.where(keep, scores, -jnp.inf)
        highest = jnp.maximum(jnp.max(scores, axis=-1, keepdims=True), sinks)
        raised = jnp.exp(scores - highest)
        denominator = jnp.sum(raised, axis=-1, keepdims=True) + jnp.exp(sinks - highest)
        weights = (raised / denominator).astype(jnp.bfloat16)
        mixed = jnp.einsum(
            "kgqs,skd->qkgd", weights, band_values, preferred_element_type=jnp.float32
        )
        outputs.append(mixed.astype(jnp.bfloat16).reshape(block_rows, heads_here * HEAD))
    return jnp.concatenate(outputs, axis=0)


def on_device(
    tokens,
    norm_gain,
    w_query,
    w_key,
    w_value,
    w_conv_in,
    w_conv_b,
    w_conv_c,
    conv_taps,
    sink_logits,
    w_attn_out,
    w_conv_out,
):
    gathered = lax.all_gather(tokens, "tp", axis=2, tiled=True)[0]
    normed = norm_rows(gathered, norm_gain)
    row_total = normed.shape[0]
    weight_rows = (
        lax.all_gather(w_query, ("sp", "fs"), axis=0, tiled=True),
        lax.all_gather(w_key, ("sp", "fs"), axis=0, tiled=True),
        lax.all_gather(w_value, ("sp", "fs"), axis=0, tiled=True),
        lax.all_gather(w_conv_in, ("sp", "fs"), axis=0, tiled=True),
        lax.all_gather(w_conv_b, ("sp", "fs"), axis=0, tiled=True),
        lax.all_gather(w_conv_c, ("sp", "fs"), axis=0, tiled=True),
    )
    results = tuple(
        (
            jnp.dot(normed, rows_part, preferred_element_type=jnp.float32)
            for rows_part in weight_rows
        )
    )
    queries, keys, values, inner, gate_b, gate_c = tuple(
        (result.astype(jnp.bfloat16) for result in results)
    )
    product = (gate_c.astype(jnp.float32) * inner.astype(jnp.float32)).astype(jnp.bfloat16)
    keys_values = jnp.concatenate([keys, values], axis=1)
    earlier_kv, earlier_product = shifted(
        (keys_values[row_total - WINDOW :], product[row_total - 2 :]), "sp", 1
    )
    heads_here = queries.shape[1] // HEAD
    head_base = lax.axis_index("tp") * heads_here
    row_base = lax.axis_index("sp") * row_total
    attended = attend(queries, keys_values, earlier_kv, sink_logits, head_base, row_base)
    taps = conv_taps.astype(jnp.float32)
    padded = jnp.concatenate([earlier_product, product], axis=0).astype(jnp.float32)
    filtered = (
        taps[0] * padded[0:row_total]
        + taps[1] * padded[1 : row_total + 1]
        + taps[2] * padded[2 : row_total + 2]
    )
    conv_out = (gate_b.astype(jnp.float32) * filtered).astype(jnp.bfloat16)
    attn_columns, conv_columns = (
        lax.all_gather(w_attn_out, ("sp", "fs"), axis=1, tiled=True),
        lax.all_gather(w_conv_out, ("sp", "fs"), axis=1, tiled=True),
    )
    summed = lax.psum_scatter(
        (
            jnp.dot(attended, attn_columns, preferred_element_type=jnp.float32)
            + jnp.dot(conv_out, conv_columns, preferred_element_type=jnp.float32)
        ).astype(jnp.bfloat16),
        "tp",
        scatter_dimension=0,
        tiled=True,
    )
    return summed[None]


def solution(mesh):
    placed = (
        P("fs", "sp", "tp"),
        P(),
        P(("sp", "fs"), "tp"),
        P(("sp", "fs"), "tp"),
        P(("sp", "fs"), "tp"),
        P(("sp", "fs"), "tp"),
        P(("sp", "fs"), "tp"),
        P(("sp", "fs"), "tp"),
        P(None, "tp"),
        P("tp"),
        P("tp", ("sp", "fs")),
        P("tp", ("sp", "fs")),
    )
    return jax.shard_map(
        on_device,
        mesh=mesh,
        in_specs=placed,
        out_specs=P("fs", ("sp", "tp"), None),
        check_vma=False,
    )
```

profile of v0, /device:TPU:0, one launch (start us, length us, event | category | flops | bytes accessed | tf_op | source)
XLA Modules:
  0.0 474.1 jit_solution(1467473243379715403)
XLA Ops:
  6.5 0.7 all-gather.10.cloned.1.call-update
  7.3 0.7 all-gather.14.cloned.1.call-update
  10.5 0.7 all-gather.18.cloned.1.call-update
  13.6 54.7 %all-gather.10.cloned.1.call-done = bf16[1,1024,2048]{2,1,0:T(8,128)(2,1)} async-done(((bf16[1,1024,1024]{2,1,0:T(8,128)(2,1)}), bf16[1,1024,2048]{2,1,0:T(8,128)(2,1)}) %all-gather.10.cloned.1.call-update) | async-done | bytes 4194320 | tf_op jit(solution)/shard_map/all_gather | solution.py:82
  68.4 3.0 convert_reduce_fusion
  71.8 1.2 fusion.7
  73.1 2.9 fusion.9
  76.0 32.4 %all-gather.14.cloned.1.call-done = bf16[2048,256]{1,0:T(8,128)(2,1)} async-done(((bf16[128,256]{1,0:T(8,128)(2,1)}), bf16[2048,256]{1,0:T(8,128)(2,1)}) %all-gather.14.cloned.1.call-update) | async-done | bytes 1048592 | tf_op jit(solution)/shard_map/all_gather | solution.py:88
  108.4 3.8 convolution_convert_fusion.4
  112.2 35.3 %all-gather.12.cloned.1.call-done = bf16[2048,256]{1,0:T(8,128)(2,1)} async-done(((bf16[128,256]{1,0:T(8,128)(2,1)}), bf16[2048,256]{1,0:T(8,128)(2,1)}) %all-gather.12.cloned.1.call-update) | async-done | bytes 1048592 | tf_op jit(solution)/shard_map/all_gather | solution.py:87
  147.5 3.8 convolution_convert_fusion.5
  151.3 2.4 collective-permute-start
  153.7 36.2 %all-gather.24.cloned.1.call-done = bf16[2048,512]{1,0:T(8,128)(2,1)} async-done(((bf16[128,512]{1,0:T(8,128)(2,1)}), bf16[2048,512]{1,0:T(8,128)(2,1)}) %all-gather.24.cloned.1.call-update) | async-done | bytes 2097168 | tf_op jit(solution)/shard_map/all_gather | solution.py:89
  189.9 6.2 %convolution_convert_fusion = bf16[1024,512]{1,0:T(8,128)(2,1)} fusion(bf16[1024,2048]{1,0:T(8,128)(2,1)} %fusion.9, bf16[2048,512]{1,0:T(8,128)(2,1)} %all-gather.24.cloned.1.call-done), kind=kOutput, calls=%fused_computation.31 | convolution fusion | flops 2148007936 | bytes 7340032 | tf_op jit(solution)/shard_map/dot_general | solution.py:95
  196.1 36.1 %all-gather.22.cloned.1.call-done = bf16[2048,512]{1,0:T(8,128)(2,1)} async-done(((bf16[128,512]{1,0:T(8,128)(2,1)}), bf16[2048,512]{1,0:T(8,128)(2,1)}) %all-gather.22.cloned.1.call-update) | async-done | bytes 2097168 | tf_op jit(solution)/shard_map/all_gather | solution.py:91
  232.1 5.5 %multiply_convert_fusion = bf16[1024,512]{1,0:T(8,128)(2,1)S(1)} fusion(bf16[1024,512]{1,0:T(8,128)(2,1)} %convolution_convert_fusion, bf16[1024,2048]{1,0:T(8,128)(2,1)} %fusion.9, bf16[2048,512]{1,0:T(8,128)(2,1)} %all-gather.22.cloned.1.call-done), kind=kOutput, calls=%fused_computation.30 | convolution fusion | flops 2150105088 | bytes 8388608 | tf_op jit(solution)/shard_map/dot_general | solution.py:95
  237.6 1.0 copy-done.2
  238.6 2.4 collective-permute-start.1
  241.0 33.4 %all-gather.16.cloned.1.call-done = bf16[2048,512]{1,0:T(8,128)(2,1)} async-done(((bf16[128,512]{1,0:T(8,128)(2,1)}), bf16[2048,512]{1,0:T(8,128)(2,1)}) %all-gather.16.cloned.1.call-update) | async-done | bytes 2097168 | tf_op jit(solution)/shard_map/all_gather | solution.py:86
  274.4 5.3 %convolution_convert_fusion.3 = bf16[1024,512]{0,1:T(8,128)(2,1)S(1)} fusion(bf16[1024,2048]{1,0:T(8,128)(2,1)} %fusion.9, bf16[2048,512]{1,0:T(8,128)(2,1)} %all-gather.16.cloned.1.call-done), kind=kOutput, calls=%fused_computation.34 | convolution fusion | flops 2148007936 | bytes 7340032 | tf_op jit(solution)/shard_map/dot_general | solution.py:95
  279.8 1.6 maximum_convert_fusion
  281.6 5.8 %fusion.11 = (f32[4,2,512]{2,1,0:T(2,128)S(1)}, f32[4,640,512,2]{2,1,3,0:T(8,128)}) fusion(f32[512,640]{0,1:T(8,128)S(1)} %fusion.18, f32[4,2]{1,0:T(4,128)S(1)} %multiply_exponential_fusion, pred[512,640]{0,1:T(8,128)(4,1)S(1)} %get-tuple-element.19, bf16[640,4,64,1]{0,2,3,1:T(8,128)(2,1)S(1)} %bitcast.93, bf16[512,4,2,64]{0,3,2,1:T(8,128)(2,1)S(1)} %bitcast.89), kind=kOutput, calls=%fused_computation.20 | convolution fusion | flops 348647424 | bytes 12992544 | tf_op jit(solution)/shard_map/qkgd,skd->kgqs/dot_general | solution.py:50
  287.4 8.4 %fusion.2 = (f32[4,2,512]{2,1,0:T(2,128)S(1)}, f32[4,2,512]{2,1,0:T(2,128)S(1)}, f32[4,640,512,2]{2,1,3,0:T(8,128)S(1)}) fusion(f32[4,640,512,2]{2,1,3,0:T(8,128)} %get-tuple-element.21, f32[4,2,512]{2,1,0:T(2,128)S(1)} %broadcast_maximum_fusion.1, f32[512,640]{0,1:T(8,128)S(1)} %fusion.18, f32[4,2]{1,0:T(4,128)S(1)} %multiply_exponential_fusion, ...), kind=kOutput, calls=%fused_computation.10 | convolution fusion | flops 361750528 | bytes 23838752 | tf_op jit(solution)/shard_map/qkgd,skd->kgqs/dot_general | solution.py:50
  295.9 2.9 fusion.3
  298.9 8.0 %fusion.23 = bf16[4,64,2,512]{3,1,2,0:T(8,128)(2,1)S(1)} fusion(bf16[640,4,64,1]{0,2,3,1:T(8,128)(2,1)S(1)} %bitcast.91, f32[4,640,512,2]{2,1,3,0:T(8,128)} %get-tuple-element.21, f32[4,2,512]{2,1,0:T(2,128)S(1)} %get-tuple-element.16, f32[4,2,512]{2,1,0:T(2,128)S(1)} %broadcast_maximum_fusion.1, f32[512,640]{0,1:T(8,128)S(1)} %fusion.18, ...), kind=kOutput, calls=%fused_computation.43 | convolution fusion | flops 354156544 | bytes 13008928 | tf_op jit(solution)/shard_map/kgqs,skd->qkgd/dot_general | solution.py:61
  306.9 4.0 fusion.22
  310.9 5.4 %all-gather.18.cloned.1.call-done = bf16[512,2048]{1,0:T(8,128)(2,1)} async-done(((bf16[512,128]{1,0:T(8,128)(2,1)}), bf16[512,2048]{1,0:T(8,128)(2,1)}) %all-gather.18.cloned.1.call-update) | async-done | bytes 2097168 | tf_op jit(solution)/shard_map/all_gather | solution.py:120
  316.3 7.4 %fusion.24 = f32[1024,2048]{1,0:T(8,128)} fusion(bf16[512,2048]{1,0:T(8,128)(2,1)} %all-gather.18.cloned.1.call-done, bf16[512,512]{0,1:T(8,128)(2,1)S(1)} %bitcast.98, bf16[512,512]{0,1:T(8,128)(2,1)S(1)} %bitcast.97), kind=kOutput, calls=%fused_computation.45 | convolution fusion | flops 2149580800 | bytes 11534336 | tf_op jit(solution)/shard_map/dot_general | solution.py:125
  323.7 35.3 %all-gather.20.cloned.1.call-done = bf16[2048,512]{1,0:T(8,128)(2,1)} async-done(((bf16[128,512]{1,0:T(8,128)(2,1)}), bf16[2048,512]{1,0:T(8,128)(2,1)}) %all-gather.20.cloned.1.call-update) | async-done | bytes 2097168 | tf_op jit(solution)/shard_map/all_gather | solution.py:90
  359.0 42.0 %all-gather.26.cloned.1.call-done = bf16[512,2048]{1,0:T(8,128)(2,1)} async-done(((bf16[512,128]{1,0:T(8,128)(2,1)}), bf16[512,2048]{1,0:T(8,128)(2,1)}) %all-gather.26.cloned.1.call-update) | async-done | bytes 2097168 | tf_op jit(solution)/shard_map/all_gather | solution.py:121
  401.0 12.6 %add_convert_fusion = bf16[1024,2048]{1,0:T(8,128)(2,1)} fusion(f32[1024,2048]{1,0:T(8,128)} %fusion.24, bf16[512,2048]{1,0:T(8,128)(2,1)} %all-gather.26.cloned.1.call-done, f32[1026,512]{1,0:T(8,128)S(1)} %copy-done.1, bf16[1024,2048]{1,0:T(8,128)(2,1)} %fusion.9, bf16[2048,512]{1,0:T(8,128)(2,1)} %all-gather.20.cloned.1.call-done, f32[512]{0:T(512)S(1)} %bitcast.96, ...), kind=kOutput, calls=%fused_computation.18 | convolution fusion | flops 4303880192 | bytes 27269120 | tf_op jit(solution)/shard_map/dot_general | solution.py:126
  413.6 53.6 %reduce-scatter.2.cloned.1.call-done = bf16[512,2048]{1,0:T(8,128)(2,1)} async-done(((bf16[1024,2048]{1,0:T(8,128)(2,1)}), bf16[512,2048]{1,0:T(8,128)(2,1)}) %reduce-scatter.2.cloned.1.call-update) | async-done | bytes 2097168 | tf_op jit(solution)/shard_map/reduce_scatter | solution.py:123
  (48 shorter events, 5.8 us)
Async XLA Ops:
  6.5 6.5 %copy-start.6 = (f32[8]{0:T(128)S(1)}, f32[8]{0:T(128)}, u32[]{:S(2)}) copy-start(f32[8]{0:T(128)} %param.21) | copy-start | bytes 100
  6.5 6.5 %copy-start.4 = (bf16[3,512]{1,0:T(4,128)(2,1)S(1)}, bf16[3,512]{1,0:T(4,128)(2,1)}, u32[]{:S(2)}) copy-start(bf16[3,512]{1,0:T(4,128)(2,1)} %param.20) | copy-start | bytes 9220
  6.5 61.8 %all-gather.10.cloned.1.call-start = ((), (), s32[]{:S(2)}) async-start(), calls=%async_computation.1 | async-start | bytes 6291456 | tf_op jit(solution)/shard_map/all_gather | solution.py:82
  7.3 101.2 %all-gather.14.cloned.1.call-start = ((), (), s32[]{:S(2)}) async-start(), calls=%async_computation.3 | async-start | bytes 1114112 | tf_op jit(solution)/shard_map/all_gather | solution.py:88
  8.0 139.4 %all-gather.12.cloned.1.call-start = ((), (), s32[]{:S(2)}) async-start(), calls=%async_computation.2 | async-start | bytes 1114112 | tf_op jit(solution)/shard_map/all_gather | solution.py:87
  8.7 181.2 %all-gather.24.cloned.1.call-start = ((), (), s32[]{:S(2)}) async-start(), calls=%async_computation.8 | async-start | bytes 2228224 | tf_op jit(solution)/shard_map/all_gather | solution.py:89
  9.3 222.8 %all-gather.22.cloned.1.call-start = ((), (), s32[]{:S(2)}) async-start(), calls=%async_computation.7 | async-start | bytes 2228224 | tf_op jit(solution)/shard_map/all_gather | solution.py:91
  9.9 264.5 %all-gather.16.cloned.1.call-start = ((), (), s32[]{:S(2)}) async-start(), calls=%async_computation.4 | async-start | bytes 2228224 | tf_op jit(solution)/shard_map/all_gather | solution.py:86
  10.5 305.8 %all-gather.18.cloned.1.call-start = ((), (), s32[]{:S(2)}) async-start(), calls=%async_computation.5 | async-start | bytes 2228224 | tf_op jit(solution)/shard_map/all_gather | solution.py:120
  11.2 347.8 %all-gather.20.cloned.1.call-start = ((), (), s32[]{:S(2)}) async-start(), calls=%async_computation.6 | async-start | bytes 2228224 | tf_op jit(solution)/shard_map/all_gather | solution.py:90
  12.0 389.0 %all-gather.26.cloned.1.call-start = ((), (), s32[]{:S(2)}) async-start(), calls=%async_computation.9 | async-start | bytes 2228224 | tf_op jit(solution)/shard_map/all_gather | solution.py:121
  12.7 454.5 %reduce-scatter.2.cloned.1.call-start = ((), (), s32[]{:S(2)}) async-start(), calls=%async_computation.10 | async-start | bytes 6291456 | tf_op jit(solution)/shard_map/reduce_scatter | solution.py:123
  13.6 59.4 %copy-start.5 = (f32[2048]{0:T(1024)S(1)}, f32[2048]{0:T(1024)}, u32[]{:S(2)}) copy-start(f32[2048]{0:T(1024)} %param.13) | copy-start | bytes 24580
  68.4 3.4 copy-start
  151.3 130.1 %collective-permute-start = (bf16[128,512]{0,1:T(8,128)(2,1)S(1)}, bf16[128,512]{0,1:T(8,128)(2,1)S(1)}, u32[]{:S(2)}, u32[]{:S(2)}) collective-permute-start(bf16[128,512]{0,1:T(8,128)(2,1)S(1)} %pad_maximum_fusion.3), channel_id=1, source_target_pairs={{0,8},{8,16},{16,24},{1,9},{9,17},{17,25},{2,10},{10,18},{18,26},{... | collective-permute-start | bytes 393224 | tf_op jit(solution)/shard_map/ppermute | solution.py:14
  237.6 1.0 copy-start.2
  238.6 41.2 %collective-permute-start.1 = (bf16[2,512]{1,0:T(2,128)(2,1)S(1)}, bf16[2,512]{1,0:T(2,128)(2,1)S(1)}, u32[]{:S(2)}, u32[]{:S(2)}) collective-permute-start(bf16[2,512]{1,0:T(2,128)(2,1)S(1)} %slice.69), channel_id=1, source_target_pairs={{0,8},{8,16},{16,24},{1,9},{9,17},{17,25},{2,10},{10,18},{18,26},{... | collective-permute-start | bytes 6152 | tf_op jit(solution)/shard_map/ppermute | solution.py:14
  274.4 5.4 %copy-start.3 = (bf16[1024,512]{1,0:T(8,128)(2,1)S(1)}, bf16[1024,512]{1,0:T(8,128)(2,1)}, u32[]{:S(2)}) copy-start(bf16[1024,512]{1,0:T(8,128)(2,1)} %copy-done.2) | copy-start | bytes 3145732
  316.3 84.7 %copy-start.1 = (f32[1026,512]{1,0:T(8,128)S(1)}, f32[1026,512]{1,0:T(8,128)}, u32[]{:S(2)}) copy-start(f32[1026,512]{1,0:T(8,128)} %maximum_convert_fusion) | copy-start | bytes 6303748
Sparse Core Ops, SparseCore 0:
  8.9 59.4 all-gather.9
  70.5 37.8 all-gather.13
  110.6 36.8 all-gather.11
  149.5 40.4 all-gather.23
  191.9 40.1 all-gather.21
  234.2 40.1 all-gather.15
  276.5 39.7 all-gather.17
  318.5 40.5 all-gather.19
  361.2 39.7 all-gather.25
  413.7 53.4 reduce-scatter.1
where the time goes:
time: 474 us
  waiting for transfers between devices  370 us (78%)
  matrix products  70.7 us (15%)
  between operations  13.7 us (3%)
  other arithmetic  12.8 us (3%)
  starting transfers between devices  5.16 us (1%)
    all_gather x1, waiting for transfers between devices, on_device(): gathered = lax.all_gather(tokens, 'tp', axis=2, tiled=True)[0]  54.7 us
    reduce_scatter x1, waiting for transfers between devices, on_device(): lax.psum_scatter((jnp.dot(attended, attn_columns, preferred_element_type=...  53.6 us
    all_gather x1, waiting for transfers between devices, on_device(): lax.all_gather(w_conv_out, ('sp', 'fs'), axis=1, tiled=True)  42 us
    all_gather x1, waiting for transfers between devices, on_device(): lax.all_gather(w_conv_in, ('sp', 'fs'), axis=0, tiled=True)  36.2 us
    all_gather x1, waiting for transfers between devices, on_device(): lax.all_gather(w_conv_c, ('sp', 'fs'), axis=0, tiled=True)  36.1 us
    all_gather x1, waiting for transfers between devices, on_device(): lax.all_gather(w_conv_b, ('sp', 'fs'), axis=0, tiled=True)  35.3 us
    all_gather x1, waiting for transfers between devices, on_device(): lax.all_gather(w_key, ('sp', 'fs'), axis=0, tiled=True)  35.3 us
    all_gather x1, waiting for transfers between devices, on_device(): lax.all_gather(w_query, ('sp', 'fs'), axis=0, tiled=True)  33.4 us
  transfers between devices with their start and end apart: 12, of which 10 were waited for; matrix products, arithmetic and copies ran while one was open for 15% of the time, Pallas kernels for 0%

commit v1 on v0

--- a/solution.py
+++ b/solution.py
@@ -1,11 +1,173 @@
+import functools
+
 import jax
 import jax.numpy as jnp
 from jax import lax
+from jax.experimental import pallas as pl
+from jax.experimental.pallas import tpu as pltpu
 from jax.sharding import PartitionSpec as P
 
 HEADS = 16
 HEAD = 64
 WINDOW = 128
+MESH = pl.DeviceIdType.MESH
+Z_FIRST = (True, False, True)
+
+
+class Gather:
+    def __init__(self, ring, fs, parts):
+        self.ring, self.outer, self.parts = ring, fs // 2, parts
+
+    def sends(self, part, key):
+        d, o, i = key
+        if i == 1:
+            return []
+        out = []
+        heavy_right = (part // 2 + o) % 2 == 0
+        right = self.ring // 2 if heavy_right else (self.ring - 1) // 2
+        left = self.ring - 1 - right
+        if Z_FIRST[part]:
+            on_ring, on_outer = o == 0, o == 0
+        else:
+            on_ring, on_outer = True, o == 0 and d == 0
+        if on_ring:
+            if d < right:
+                out.append(("right", (d + 1, o, 0)))
+            if d == 0 and left > 0:
+                out.append(("left", (self.ring - 1, o, 0)))
+            elif d > right and self.ring - d < left:
+                out.append(("left", (d - 1, o, 0)))
+        if on_outer:
+            for step in range(1, self.outer):
+                out.append((("outer", step), (d, step, 0)))
+        out.append(("core", (d, o, 1)))
+        return out
+
+    def plan(self):
+        order, level = [], {}
+        frontier = [(0, part, (0, 0, 0)) for part in range(self.parts)]
+        while frontier:
+            frontier.sort()
+            hops, part, key = frontier.pop(0)
+            order.append((part, key, self.sends(part, key)))
+            for _, there in self.sends(part, key):
+                frontier.append((hops + 1, part, there))
+        return order
+
+
+def gather_kernel(gather, n_tp, *refs):
+    parts = gather.parts
+    own = refs[:parts]
+    tok = refs[parts]
+    full = refs[parts + 1 : 2 * parts + 1]
+    tok_full = refs[2 * parts + 1]
+    send_sem, recv_sem, local_sem, tok_send, tok_recv = refs[2 * parts + 2 :]
+    n_sp, n_out = gather.ring, gather.outer
+    s, f, t = lax.axis_index("sp"), lax.axis_index("fs"), lax.axis_index("tp")
+    o, i = f // 2, f % 2
+
+    def device(where):
+        if where == "right":
+            return (lax.rem(s + 1, n_sp), f, t)
+        if where == "left":
+            return (lax.rem(s + n_sp - 1, n_sp), f, t)
+        if where == "core":
+            return (s, o * 2 + (1 - i), t)
+        if where[0] == "outer":
+            return (s, lax.rem(o + where[1], n_out) * 2 + i, t)
+        return (s, f, lax.rem(t + where[1], n_tp))
+
+    barrier = pltpu.get_barrier_semaphore()
+    greeted = ["right", "left", "core"]
+    greeted += [("outer", k) for k in range(1, n_out)] + [("tp", k) for k in range(1, n_tp)]
+    for where in greeted:
+        pl.semaphore_signal(barrier, inc=1, device_id=device(where), device_id_type=MESH)
+    pl.semaphore_wait(barrier, len(greeted))
+
+    def origin(key):
+        d, od, c = key
+        src_s = lax.rem(s + n_sp - d, n_sp)
+        src_o = lax.rem(o + n_out - od, n_out)
+        src_i = i if c == 0 else 1 - i
+        return src_s * (2 * n_out) + src_o * 2 + src_i
+
+    cols = tok.shape[1]
+    tok_copies = []
+    for k in range(1, n_tp):
+        copy = pltpu.make_async_remote_copy(
+            src_ref=tok,
+            dst_ref=tok_full.at[:, pl.ds(pl.multiple_of(t * cols, cols), cols)],
+            send_sem=tok_send.at[k],
+            recv_sem=tok_recv.at[k],
+            device_id=device(("tp", k)),
+            device_id_type=MESH,
+        )
+        copy.start()
+        tok_copies.append(copy)
+    flat = lambda key: (key[0] * n_out + key[1]) * 2 + key[2]
+    copies, arrived, last = [], {}, []
+    for part, key, sends in gather.plan():
+        rows = own[part].shape[0]
+        place = full[part].at[pl.ds(pl.multiple_of(origin(key) * rows, rows), rows)]
+        if key == (0, 0, 0):
+            source = own[part]
+        else:
+            source = place
+            if sends:
+                arrived[(part, key)].wait_recv()
+            else:
+                last.append(arrived[(part, key)])
+        for where, there in sends:
+            copy = pltpu.make_async_remote_copy(
+                src_ref=source,
+                dst_ref=place,
+                send_sem=send_sem.at[len(copies)],
+                recv_sem=recv_sem.at[part * 2 * n_sp * n_out + flat(there)],
+                device_id=device(where),
+                device_id_type=MESH,
+            )
+            copy.start()
+            copies.append(copy)
+            arrived[(part, there)] = copy
+    local = []
+    for part in range(parts):
+        rows = own[part].shape[0]
+        mine = pl.ds(pl.multiple_of(origin((0, 0, 0)) * rows, rows), rows)
+        local.append(pltpu.make_async_copy(own[part], full[part].at[mine], local_sem.at[part]))
+    mine = pl.ds(pl.multiple_of(t * cols, cols), cols)
+    local.append(pltpu.make_async_copy(tok, tok_full.at[:, mine], local_sem.at[parts]))
+    for copy in local:
+        copy.start()
+    for copy in last:
+        copy.wait_recv()
+    for copy in tok_copies:
+        copy.wait()
+    for copy in copies:
+        copy.wait_send()
+    for copy in local:
+        copy.wait()
+
+
+def gather_all(tokens, blocks):
+    n_sp, n_fs, n_tp = (lax.axis_size(axis) for axis in ("sp", "fs", "tp"))
+    gather = Gather(n_sp, n_fs, len(blocks))
+    number = sum(len(sends) for _, _, sends in gather.plan())
+    shapes = [jax.ShapeDtypeStruct((n_sp * n_fs * b.shape[0], b.shape[1]), b.dtype) for b in blocks]
+    shapes.append(jax.ShapeDtypeStruct((tokens.shape[0], tokens.shape[1] * n_tp), tokens.dtype))
+    return pl.pallas_call(
+        functools.partial(gather_kernel, gather, n_tp),
+        out_shape=shapes,
+        in_specs=[pl.BlockSpec(memory_space=pl.ANY)] * (len(blocks) + 1),
+        out_specs=[pl.BlockSpec(memory_space=pl.ANY)] * len(shapes),
+        scratch_shapes=[
+            pltpu.SemaphoreType.DMA((number,)),
+            pltpu.SemaphoreType.DMA((len(blocks) * n_sp * n_fs,)),
+            pltpu.SemaphoreType.DMA((len(blocks) + 1,)),
+            pltpu.SemaphoreType.DMA((n_tp,)),
+            pltpu.SemaphoreType.DMA((n_tp,)),
+        ],
+        compiler_params=pltpu.CompilerParams(collective_id=0, has_side_effects=True),
+    )(*blocks, tokens)
 
 
 def shifted(block, axis, distance):
@@ -79,28 +241,20 @@
     w_attn_out,
     w_conv_out,
 ):
-    gathered = lax.all_gather(tokens, "tp", axis=2, tiled=True)[0]
+    blocks = (
+        jnp.concatenate([w_query, w_key, w_value], axis=1),
+        jnp.concatenate([w_conv_in, w_conv_b, w_conv_c], axis=1),
+        jnp.concatenate([w_attn_out, w_conv_out], axis=0).T,
+    )
+    w_qkv, w_conv, w_out, gathered = gather_all(tokens[0], blocks)
     normed = norm_rows(gathered, norm_gain)
     row_total = normed.shape[0]
-    weight_rows = (
-        lax.all_gather(w_query, ("sp", "fs"), axis=0, tiled=True),
-        lax.all_gather(w_key, ("sp", "fs"), axis=0, tiled=True),
-        lax.all_gather(w_value, ("sp", "fs"), axis=0, tiled=True),
-        lax.all_gather(w_conv_in, ("sp", "fs"), axis=0, tiled=True),
-        lax.all_gather(w_conv_b, ("sp", "fs"), axis=0, tiled=True),
-        lax.all_gather(w_conv_c, ("sp", "fs"), axis=0, tiled=True),
-    )
-    results = tuple(
-        (
-            jnp.dot(normed, rows_part, preferred_element_type=jnp.float32)
-            for rows_part in weight_rows
-        )
-    )
-    queries, keys, values, inner, gate_b, gate_c = tuple(
-        (result.astype(jnp.bfloat16) for result in results)
-    )
+    q_cols, kv_cols, conv_cols = w_query.shape[1], w_key.shape[1], w_conv_in.shape[1]
+    qkv = jnp.dot(normed, w_qkv, preferred_element_type=jnp.float32).astype(jnp.bfloat16)
+    conv = jnp.dot(normed, w_conv, preferred_element_type=jnp.float32).astype(jnp.bfloat16)
+    queries, keys_values = qkv[:, :q_cols], qkv[:, q_cols:]
+    inner, gate_b, gate_c = (conv[:, k * conv_cols : (k + 1) * conv_cols] for k in range(3))
     product = (gate_c.astype(jnp.float32) * inner.astype(jnp.float32)).astype(jnp.bfloat16)
-    keys_values = jnp.concatenate([keys, values], axis=1)
     earlier_kv, earlier_product = shifted(
         (keys_values[row_total - WINDOW :], product[row_total - 2 :]), "sp", 1
     )
@@ -116,19 +270,11 @@
         + taps[2] * padded[2 : row_total + 2]
     )
     conv_out = (gate_b.astype(jnp.float32) * filtered).astype(jnp.bfloat16)
-    attn_columns, conv_columns = (
-        lax.all_gather(w_attn_out, ("sp", "fs"), axis=1, tiled=True),
-        lax.all_gather(w_conv_out, ("sp", "fs"), axis=1, tiled=True),
-    )
-    summed = lax.psum_scatter(
-        (
-            jnp.dot(attended, attn_columns, preferred_element_type=jnp.float32)
-            + jnp.dot(conv_out, conv_columns, preferred_element_type=jnp.float32)
-        ).astype(jnp.bfloat16),
-        "tp",
-        scatter_dimension=0,
-        tiled=True,
-    )
+    mixers = jnp.concatenate([attended, conv_out], axis=1)
+    partial = lax.dot_general(
+        mixers, w_out, (((1,), (1,)), ((), ())), preferred_element_type=jnp.float32
+    ).astype(jnp.bfloat16)
+    summed = lax.psum_scatter(partial, "tp", scatter_dimension=0, tiled=True)
     return summed[None]
 
 

time: 474 us -> 336 us (0.71)
  waiting for transfers between devices: 370 us -> 54.1 us
  Pallas kernels: 0 us -> 183 us
  matrix products: 70.7 us -> 44.7 us
  other arithmetic: 12.8 us -> 21.7 us
  local copies, waits for them, and re-layouts: 1.63 us -> 10.4 us
    all_gather x9 -> x0, waiting for transfers between devices: 311 us -> none  [the longest x1 54.7 us: on_device(): gathered = lax.all_gather(tokens, 'tp', axis=2, tiled=True)[0]]
    pallas_call x0 -> x1, Pallas kernels: none -> 183 us  [gather_all(): pl.pallas_call(functools.partial(gather_kernel, gather, n_tp), out_shape=...]
    dot_general x7 -> x3, matrix products: 44.5 us -> 24.6 us  [the longest x1 11.7 us: on_device(): lax.dot_general(mixers, w_out, (((1,), (1,)), ((), ())), preferred_elemen...]
    unnamed x10 -> x1, waiting for transfers between devices: 5.76 us -> 0.02 us
  transfers between devices with their start and end apart: 12 -> 3, of which waited for: 10 -> 1; matrix products, arithmetic and copies ran while one was open for 15% -> 5% of each run, Pallas kernels for 0% -> 0%
where the time goes in v1:
time: 336 us; the launch traced here: 335 us
  Pallas kernels  183 us (54%)
  waiting for transfers between devices  54.1 us (16%)
  matrix products  44.7 us (13%)
  other arithmetic  21.7 us (6%)
  between operations  13.7 us (4%)
  local copies, waits for them, and re-layouts  10.4 us (3%)
  starting transfers between devices  7.66 us (2%)
    pallas_call x1, Pallas kernels, gather_all(): pl.pallas_call(functools.partial(gather_kernel, gather, n_tp), out_shape=...  183 us
    reduce_scatter x1, waiting for transfers between devices, on_device(): summed = lax.psum_scatter(partial, 'tp', scatter_dimension=0, tiled=True)  54.1 us
    dot_general x2, matrix products, attend(): jnp.einsum('qkgd,skd->kgqs', query_block, band_keys, preferred_element_ty...  11.8 us
    dot_general x1, matrix products, on_device(): lax.dot_general(mixers, w_out, (((1,), (1,)), ((), ())), preferred_elemen...  11.7 us
    dot_general x2, matrix products, attend(): jnp.einsum('kgqs,skd->qkgd', weights, band_values, preferred_element_type...  8.3 us
    ppermute x2, starting transfers between devices, shifted(): return lax.ppermute(block, axis, route)  7.66 us
    dot_general x1, matrix products, on_device(): jnp.dot(normed, w_conv, preferred_element_type=jnp.float32)  7.33 us
    reduce_sum x1, other arithmetic, attend(): jnp.sum(raised, axis=-1, keepdims=True) + jnp.exp(sinks - highest)  7.01 us
  transfers between devices with their start and end apart: 3, of which 1 were waited for; matrix products, arithmetic and copies ran while one was open for 5% of the time, Pallas kernels for 0%

profile of v1, /device:TPU:0, one launch (start us, length us, event | category | flops | bytes accessed | tf_op | source)
XLA Modules:
  0.0 335.2 jit_solution(1212535822963636656)
XLA Ops:
  6.5 1.0 copy.19
  7.5 1.0 copy.20
  8.6 0.7 maximum_bitcast_fusion.refs_2_
  9.3 1.7 pad_maximum_fusion.3.refs_0_
  11.0 1.8 pad_maximum_fusion.refs_1_
  12.8 183.0 %shard_map.118 = (bf16[2048,1024]{1,0:T(8,128)(2,1)}, bf16[2048,1536]{1,0:T(8,128)(2,1)}, bf16[2048,1024]{1,0:T(8,128)(2,1)}, bf16[1024,2048]{1,0:T(8,128)(2,1)}) custom-call(bf16[128,1024]{1,0:T(8,128)(2,1)} %pad_maximum_fusion.3.refs_0_, bf16[128,1536]{1,0:T(8,128)(2,1)} %pad_maximum_fusion.refs_1_, bf16[128,1024]{1,0:T(8,128)(2,1)} %maximum_bitcast_fusion.refs_2_, ...), custom_call_target="tpu_custom_call" | custom-call | tf_op jit(solution)/shard_map/pallas_call | solution.py:157
  195.8 3.0 convert_reduce_fusion
  198.8 0.5 copy-done
  199.3 1.2 fusion.6
  200.5 5.5 %convolution_convert_fusion.2 = bf16[1024,1024]{0,1:T(8,128)(2,1)S(1)} fusion(bf16[2048,1024]{1,0:T(8,128)(2,1)S(1)} %copy-done.12, bf16[1024,2048]{1,0:T(8,128)(2,1)S(1)} %copy-done, f32[2048]{0:T(1024)S(1)} %copy-done.13, f32[1024]{0:T(1024)S(1)} %add_rsqrt_fusion, f32[1024]{0:T(1024)S(1)} %broadcast_multiply_fusion), kind=kOutput, calls=%fused_computation.36 | convolution fusion | flops 4306501632 | bytes 10502144 | tf_op jit(solution)/shard_map/dot_general | solution.py:253
  206.1 0.8 slice.83
  206.9 3.5 %collective-permute-start = (bf16[128,512]{0,1:T(8,128)(2,1)}, bf16[128,512]{0,1:T(8,128)(2,1)S(1)}, u32[]{:S(2)}, u32[]{:S(2)}) collective-permute-start(bf16[128,512]{0,1:T(8,128)(2,1)} %slice.83), channel_id=1, source_target_pairs={{0,8},{8,16},{16,24},{1,9},{9,17},{17,25},{2,10},{10,18},{18,26},{... | collective-permute-start | bytes 393224 | tf_op jit(solution)/shard_map/ppermute | solution.py:176
  210.4 7.3 %convolution_convert_fusion = bf16[1024,1536]{1,0:T(8,128)(2,1)S(1)} fusion(bf16[2048,1536]{1,0:T(8,128)(2,1)S(1)} %bitcast.79, bf16[1024,2048]{1,0:T(8,128)(2,1)S(1)} %copy-done, f32[2048]{0:T(1024)S(1)} %copy-done.13, f32[1024]{0:T(1024)S(1)} %add_rsqrt_fusion, f32[1024]{0:T(1024)S(1)} %broadcast_multiply_fusion), kind=kOutput, calls=%fused_computation.21 | convolution fusion | flops 6454509568 | bytes 13647872 | tf_op jit(solution)/shard_map/dot_general | solution.py:254
  217.7 1.6 copy-done.3
  219.4 0.3 multiply_convert_fusion
  219.6 0.6 slice.93
  220.2 4.2 %collective-permute-start.1 = (bf16[2,512]{1,0:T(2,128)(2,1)}, bf16[2,512]{1,0:T(2,128)(2,1)}, u32[]{:S(2)}, u32[]{:S(2)}) collective-permute-start(bf16[2,512]{1,0:T(2,128)(2,1)} %slice.93), channel_id=1, source_target_pairs={{0,8},{8,16},{16,24},{1,9},{9,17},{17,25},{2,10},{10,18},{18,26},{... | collective-permute-start | bytes 6152 | tf_op jit(solution)/shard_map/ppermute | solution.py:176
  224.4 0.9 fusion.38
  225.3 1.1 fusion.37
  226.4 0.6 fusion.39
  227.2 1.4 fusion.28
  228.6 0.8 max.32
  229.4 1.1 maximum_convert_fusion
  230.5 3.0 fusion.15
  233.6 3.2 fusion.10
  236.9 8.7 %fusion.4 = (f32[4,2,512]{2,1,0:T(2,128)S(1)}, f32[4,2,512]{2,1,0:T(2,128)S(1)}, f32[4,640,512,2]{2,1,3,0:T(8,128)}) fusion(f32[4,640,512,2]{2,1,3,0:T(8,128)S(1)} %get-tuple-element.29, f32[4,2,512]{2,1,0:T(2,128)S(1)} %broadcast_maximum_fusion.1, f32[512,640]{0,1:T(8,128)S(1)} %fusion.22, f32[4,2]{1,0:T(4,128)S(1)} %multiply_exponential_fusion, ...), kind=kOutput, calls=%fused_computation.12 | convolution fusion | flops 361750528 | bytes 23838752 | tf_op jit(solution)/shard_map/qkgd,skd->kgqs/dot_general | solution.py:212
  245.6 3.8 %fusion.27 = bf16[4,64,2,512]{3,1,2,0:T(8,128)(2,1)S(1)} fusion(bf16[640,4,64,1]{0,2,3,1:T(8,128)(2,1)S(1)} %bitcast.73, f32[4,640,512,2]{2,1,3,0:T(8,128)S(1)} %get-tuple-element.29, f32[4,2,512]{2,1,0:T(2,128)S(1)} %get-tuple-element.24, f32[4,2,512]{2,1,0:T(2,128)S(1)} %broadcast_maximum_fusion.1, f32[512,640]{0,1:T(8,128)S(1)} %fusion.22, ...), kind=kOutput, calls=%fused_computation.43 | convolution fusion | flops 354156544 | bytes 13008928 | tf_op jit(solution)/shard_map/kgqs,skd->qkgd/dot_general | solution.py:223
  249.7 7.0 %fusion.5 = f32[4,2,512]{2,1,0:T(2,128)S(1)} fusion(f32[4,640,512,2]{2,1,3,0:T(8,128)} %get-tuple-element.30, f32[4,2,512]{2,1,0:T(2,128)S(1)} %get-tuple-element.25, f32[512,640]{0,1:T(8,128)S(1)} %fusion.22, f32[4,2]{1,0:T(4,128)S(1)} %multiply_exponential_fusion, pred[512,640]{0,1:T(8,128)(4,1)S(1)} %copy-done.4), kind=kLoop, calls=%fused_computation.13 | loop fusion | flops 15724544 | bytes 12156960 | tf_op jit(solution)/shard_map/reduce_sum | solution.py:221
  256.8 4.5 %fusion.26 = bf16[4,64,2,512]{3,1,2,0:T(8,128)(2,1)} fusion(bf16[640,4,64,1]{0,2,3,1:T(8,128)(2,1)S(1)} %bitcast.71, f32[4,640,512,2]{2,1,3,0:T(8,128)S(1)} %copy-done.1, f32[4,2,512]{2,1,0:T(2,128)S(1)} %exponential_add_fusion, f32[4,2,512]{2,1,0:T(2,128)S(1)} %get-tuple-element.25, f32[512,640]{0,1:T(8,128)S(1)} %fusion.22, ...), kind=kOutput, calls=%fused_computation.42 | convolution fusion | flops 354156544 | bytes 13008928 | tf_op jit(solution)/shard_map/kgqs,skd->qkgd/dot_general | solution.py:223
  261.3 1.3 copy.24
  262.6 11.7 %convolution_convert_fusion.1 = bf16[1024,2048]{1,0:T(8,128)(2,1)} fusion(bf16[2048,1024]{1,0:T(8,128)(2,1)} %get-tuple-element.12, bf16[1024,512]{1,0:T(8,128)(2,1)S(1)} %copy-done.5, bf16[512,512]{1,0:T(8,128)(2,1)S(1)} %copy.24, bf16[512,512]{1,0:T(8,128)(2,1)S(1)} %copy.23), kind=kOutput, calls=%fused_computation.22 | convolution fusion | flops 4303355904 | bytes 10485760 | tf_op jit(solution)/shard_map/dot_general | solution.py:274
  274.3 54.1 %reduce-scatter.2.cloned.1.call-done = bf16[512,2048]{1,0:T(8,128)(2,1)} async-done(((bf16[1024,2048]{1,0:T(8,128)(2,1)}), bf16[512,2048]{1,0:T(8,128)(2,1)}) %reduce-scatter.2.cloned.1.call-update) | async-done | bytes 2097168 | tf_op jit(solution)/shard_map/reduce_scatter | solution.py:277
  (48 shorter events, 0.8 us)
Async XLA Ops:
  6.5 321.9 %reduce-scatter.2.cloned.1.call-start = ((), (), s32[]{:S(2)}) async-start(), calls=%async_computation.1 | async-start | bytes 6291456 | tf_op jit(solution)/shard_map/reduce_scatter | solution.py:277
  9.3 191.2 %copy-start.13 = (f32[2048]{0:T(1024)S(1)}, f32[2048]{0:T(1024)}, u32[]{:S(2)}) copy-start(f32[2048]{0:T(1024)} %param.13) | copy-start | bytes 24580
  195.8 3.5 %copy-start = (bf16[1024,2048]{1,0:T(8,128)(2,1)S(1)}, bf16[1024,2048]{1,0:T(8,128)(2,1)}, u32[]{:S(2)}) copy-start(bf16[1024,2048]{1,0:T(8,128)(2,1)} %get-tuple-element.9) | copy-start | bytes 12582916
  195.8 4.7 %copy-start.12 = (bf16[2048,1024]{1,0:T(8,128)(2,1)S(1)}, bf16[2048,1024]{1,0:T(8,128)(2,1)}, u32[]{:S(2)}) copy-start(bf16[2048,1024]{1,0:T(8,128)(2,1)} %get-tuple-element.10) | copy-start | bytes 12582916
  199.3 11.1 %slice-start.1 = ((s8[6291456]{0:T(1024)(128)(4,1)}), s8[4194304]{0:T(1024)(128)(4,1)S(1)}, s32[]{:S(2)}) async-start(s8[6291456]{0:T(1024)(128)(4,1)} %bitcast.78), calls=%async_computation.3 | async-start | bytes 8388608
  200.5 9.8 %slice-start.2 = ((s8[6291456]{0:T(1024)(128)(4,1)}), s8[2097152]{0:T(1024)(128)(4,1)S(1)}, s32[]{:S(2)}) async-start(s8[6291456]{0:T(1024)(128)(4,1)} %bitcast.78), calls=%async_computation.4 | async-start | bytes 4194304
  206.1 19.2 %copy-start.2 = (bf16[1024,1024]{0,1:T(8,128)(2,1)}, bf16[1024,1024]{0,1:T(8,128)(2,1)S(1)}, u32[]{:S(2)}) copy-start(bf16[1024,1024]{0,1:T(8,128)(2,1)S(1)} %convolution_convert_fusion.2) | copy-start | bytes 6291460
  206.9 26.6 %collective-permute-start = (bf16[128,512]{0,1:T(8,128)(2,1)}, bf16[128,512]{0,1:T(8,128)(2,1)S(1)}, u32[]{:S(2)}, u32[]{:S(2)}) collective-permute-start(bf16[128,512]{0,1:T(8,128)(2,1)} %slice.83), channel_id=1, source_target_pairs={{0,8},{8,16},{16,24},{1,9},{9,17},{17,25},{2,10},{10,18},{18,26},{... | collective-permute-start | bytes 393224 | tf_op jit(solution)/shard_map/ppermute | solution.py:176
  217.7 1.6 copy-start.3
  219.4 7.0 %copy-start.11 = (bf16[3,512]{1,0:T(4,128)(2,1)S(1)}, bf16[3,512]{1,0:T(4,128)(2,1)}, u32[]{:S(2)}) copy-start(bf16[3,512]{1,0:T(4,128)(2,1)} %param.20) | copy-start | bytes 9220
  220.2 9.2 %collective-permute-start.1 = (bf16[2,512]{1,0:T(2,128)(2,1)}, bf16[2,512]{1,0:T(2,128)(2,1)}, u32[]{:S(2)}, u32[]{:S(2)}) collective-permute-start(bf16[2,512]{1,0:T(2,128)(2,1)} %slice.93), channel_id=1, source_target_pairs={{0,8},{8,16},{16,24},{1,9},{9,17},{17,25},{2,10},{10,18},{18,26},{... | collective-permute-start | bytes 6152 | tf_op jit(solution)/shard_map/ppermute | solution.py:176
  228.6 4.9 %slice-start = ((bf16[1024,1024]{0,1:T(8,128)(2,1)}), bf16[1024,512]{0,1:T(8,128)(2,1)S(1)}, s32[]{:S(2)}) async-start(bf16[1024,1024]{0,1:T(8,128)(2,1)} %copy-done.2), calls=%async_computation.2 | async-start | bytes 2097152 | tf_op jit(solution)/shard_map/slice | solution.py:255
  229.4 4.2 %copy-start.7 = (bf16[512,512]{0,1:T(8,128)(2,1)S(1)}, bf16[512,512]{0,1:T(8,128)(2,1)}, u32[]{:S(2)}) copy-start(bf16[512,512]{0,1:T(8,128)(2,1)} %get-tuple-element.15) | copy-start | bytes 1572868
  229.4 4.2 %copy-start.10 = (pred[512,640]{0,1:T(8,128)(4,1)S(1)}, pred[512,640]{0,1:T(8,128)(4,1)}, u32[]{:S(2)}) copy-start(pred[512,640]{0,1:T(8,128)(4,1)} %get-tuple-element.27) | copy-start | bytes 983044
  233.6 3.3 copy-start.4
  233.6 3.3 copy-start.6
  233.6 3.3 copy-start.9
  249.7 7.1 %copy-start.1 = (f32[4,640,512,2]{2,1,3,0:T(8,128)S(1)}, f32[4,640,512,2]{2,1,3,0:T(8,128)}, u32[]{:S(2)}) copy-start(f32[4,640,512,2]{2,1,3,0:T(8,128)} %get-tuple-element.30) | copy-start | bytes 31457284
  249.7 7.1 %copy-start.8 = (bf16[640,256]{0,1:T(8,128)(2,1)S(1)}, bf16[640,256]{0,1:T(8,128)(2,1)}, u32[]{:S(2)}) copy-start(bf16[640,256]{0,1:T(8,128)(2,1)} %get-tuple-element.18) | copy-start | bytes 983044
  256.8 5.8 %copy-start.5 = (bf16[1024,512]{1,0:T(8,128)(2,1)S(1)}, bf16[1024,512]{1,0:T(8,128)(2,1)}, u32[]{:S(2)}) copy-start(bf16[1024,512]{1,0:T(8,128)(2,1)} %fusion.15) | copy-start | bytes 3145732
Sparse Core Ops, SparseCore 0:
  274.5 53.8 reduce-scatter.1

commit v2 on v1

--- a/solution.py
+++ b/solution.py
@@ -11,7 +11,7 @@
 HEAD = 64
 WINDOW = 128
 MESH = pl.DeviceIdType.MESH
-Z_FIRST = (True, False, True)
+Z_FIRST = (True, True, False, True)
 
 
 class Gather:
@@ -157,7 +157,7 @@
     return pl.pallas_call(
         functools.partial(gather_kernel, gather, n_tp),
         out_shape=shapes,
-        in_specs=[pl.BlockSpec(memory_space=pl.ANY)] * (len(blocks) + 1),
+        in_specs=[pl.BlockSpec(memory_space=pltpu.VMEM)] * (len(blocks) + 1),
         out_specs=[pl.BlockSpec(memory_space=pl.ANY)] * len(shapes),
         scratch_shapes=[
             pltpu.SemaphoreType.DMA((number,)),
@@ -168,6 +168,72 @@
         ],
         compiler_params=pltpu.CompilerParams(collective_id=0, has_side_effects=True),
     )(*blocks, tokens)
+
+
+def out_kernel(n_tp, chunks, mix, w_out, out, outbox, inbox, send_sem, recv_sem):
+    s, f, t = lax.axis_index("sp"), lax.axis_index("fs"), lax.axis_index("tp")
+    rows = out.shape[0]
+    step = rows // chunks
+    peers = [(s, f, lax.rem(t + k, n_tp)) for k in range(1, n_tp)]
+    barrier = pltpu.get_barrier_semaphore()
+    for peer in peers:
+        pl.semaphore_signal(barrier, inc=1, device_id=peer, device_id_type=MESH)
+    pl.semaphore_wait(barrier, n_tp - 1)
+
+    def partial(owner, chunk):
+        first = pl.multiple_of(owner * rows + chunk * step, step)
+        return lax.dot_general(
+            mix[pl.ds(first, step), :],
+            w_out[...],
+            (((1,), (1,)), ((), ())),
+            preferred_element_type=jnp.float32,
+        ).astype(jnp.bfloat16)
+
+    copies = []
+    for chunk in range(chunks):
+        here = pl.ds(chunk * step, step)
+        for k, peer in enumerate(peers):
+            outbox[k, here] = partial(peer[2], chunk)
+            copy = pltpu.make_async_remote_copy(
+                src_ref=outbox.at[k, here],
+                dst_ref=inbox.at[k, here],
+                send_sem=send_sem.at[k, chunk],
+                recv_sem=recv_sem.at[k, chunk],
+                device_id=peer,
+                device_id_type=MESH,
+            )
+            copy.start()
+            copies.append(copy)
+    for chunk in range(chunks):
+        out[pl.ds(chunk * step, step)] = partial(t, chunk)
+    for chunk in range(chunks):
+        here = pl.ds(chunk * step, step)
+        total = out[here].astype(jnp.float32)
+        for k in range(n_tp - 1):
+            copies[chunk * (n_tp - 1) + k].wait_recv()
+            total = total + inbox[k, here].astype(jnp.float32)
+        out[here] = total.astype(out.dtype)
+    for copy in copies:
+        copy.wait_send()
+
+
+def project_out(mixers, w_out):
+    n_tp = lax.axis_size("tp")
+    rows, width = mixers.shape[0] // n_tp, w_out.shape[0]
+    chunks = 4
+    return pl.pallas_call(
+        functools.partial(out_kernel, n_tp, chunks),
+        out_shape=jax.ShapeDtypeStruct((rows, width), jnp.bfloat16),
+        in_specs=[pl.BlockSpec(memory_space=pltpu.VMEM)] * 2,
+        out_specs=pl.BlockSpec(memory_space=pltpu.VMEM),
+        scratch_shapes=[
+            pltpu.VMEM((n_tp - 1, rows, width), jnp.bfloat16),
+            pltpu.VMEM((n_tp - 1, rows, width), jnp.bfloat16),
+            pltpu.SemaphoreType.DMA((n_tp - 1, chunks)),
+            pltpu.SemaphoreType.DMA((n_tp - 1, chunks)),
+        ],
+        compiler_params=pltpu.CompilerParams(collective_id=1, has_side_effects=True),
+    )(mixers, w_out)
 
 
 def shifted(block, axis, distance):
@@ -243,17 +309,19 @@
 ):
     blocks = (
         jnp.concatenate([w_query, w_key, w_value], axis=1),
-        jnp.concatenate([w_conv_in, w_conv_b, w_conv_c], axis=1),
+        jnp.concatenate([w_conv_in, w_conv_b], axis=1),
+        w_conv_c,
         jnp.concatenate([w_attn_out, w_conv_out], axis=0).T,
     )
-    w_qkv, w_conv, w_out, gathered = gather_all(tokens[0], blocks)
+    w_qkv, w_conv, w_gate, w_out, gathered = gather_all(tokens[0], blocks)
     normed = norm_rows(gathered, norm_gain)
     row_total = normed.shape[0]
     q_cols, kv_cols, conv_cols = w_query.shape[1], w_key.shape[1], w_conv_in.shape[1]
     qkv = jnp.dot(normed, w_qkv, preferred_element_type=jnp.float32).astype(jnp.bfloat16)
     conv = jnp.dot(normed, w_conv, preferred_element_type=jnp.float32).astype(jnp.bfloat16)
     queries, keys_values = qkv[:, :q_cols], qkv[:, q_cols:]
-    inner, gate_b, gate_c = (conv[:, k * conv_cols : (k + 1) * conv_cols] for k in range(3))
+    inner, gate_b = conv[:, :conv_cols], conv[:, conv_cols:]
+    gate_c = jnp.dot(normed, w_gate, preferred_element_type=jnp.float32).astype(jnp.bfloat16)
     product = (gate_c.astype(jnp.float32) * inner.astype(jnp.float32)).astype(jnp.bfloat16)
     earlier_kv, earlier_product = shifted(
         (keys_values[row_total - WINDOW :], product[row_total - 2 :]), "sp", 1
@@ -271,10 +339,7 @@
     )
     conv_out = (gate_b.astype(jnp.float32) * filtered).astype(jnp.bfloat16)
     mixers = jnp.concatenate([attended, conv_out], axis=1)
-    partial = lax.dot_general(
-        mixers, w_out, (((1,), (1,)), ((), ())), preferred_element_type=jnp.float32
-    ).astype(jnp.bfloat16)
-    summed = lax.psum_scatter(partial, "tp", scatter_dimension=0, tiled=True)
+    summed = project_out(mixers, w_out)
     return summed[None]
 
 

time: 336 us -> 212 us (0.63)
  waiting for transfers between devices: 54.1 us -> 0.01 us
  Pallas kernels: 183 us -> 135 us
  between operations: 13.7 us -> 0.38 us
  matrix products: 44.7 us -> 32.7 us
    pallas_call x1, Pallas kernels: 183 us -> 82 us  [gather_all(): pl.pallas_call(functools.partial(gather_kernel, gather, n_tp), out_shape=...]
    reduce_scatter x1 -> x0, waiting for transfers between devices: 54.1 us -> none  [on_device(): summed = lax.psum_scatter(partial, 'tp', scatter_dimension=0, tiled=True)]
    pallas_call x0 -> x1, Pallas kernels: none -> 53.2 us  [project_out(): pl.pallas_call(functools.partial(out_kernel, n_tp, chunks), out_shape=jax...]
    dot_general x1, matrix products: 11.7 us -> 2.32 us  [on_device(): jnp.dot(normed, w_gate, preferred_element_type=jnp.float32)]
  transfers between devices with their start and end apart: 3 -> 2, of which waited for: 1 -> 0; matrix products, arithmetic and copies ran while one was open for 5% -> 7% of each run, Pallas kernels for 0% -> 0%
where the time goes in v2:
time: 212 us; the launch traced here: 211 us
  Pallas kernels  135 us (64%)
  matrix products  32.7 us (15%)
  other arithmetic  22.7 us (11%)
  local copies, waits for them, and re-layouts  13.5 us (6%)
  starting transfers between devices  7.02 us (3%)
    pallas_call x1, Pallas kernels, gather_all(): pl.pallas_call(functools.partial(gather_kernel, gather, n_tp), out_shape=...  82 us
    pallas_call x1, Pallas kernels, project_out(): pl.pallas_call(functools.partial(out_kernel, n_tp, chunks), out_shape=jax...  53.2 us
    dot_general x2, matrix products, attend(): jnp.einsum('qkgd,skd->kgqs', query_block, band_keys, preferred_element_ty...  11.8 us
    dot_general x2, matrix products, attend(): jnp.einsum('kgqs,skd->qkgd', weights, band_values, preferred_element_type...  9.02 us
    ppermute x2, starting transfers between devices, shifted(): return lax.ppermute(block, axis, route)  7.02 us
    reduce_sum x1, other arithmetic, attend(): jnp.sum(raised, axis=-1, keepdims=True) + jnp.exp(sinks - highest)  7.01 us
    unnamed x35, local copies, waits for them, and re-layouts  6.23 us
    dot_general x1, matrix products, on_device(): jnp.dot(normed, w_qkv, preferred_element_type=jnp.float32)  4.82 us
  transfers between devices with their start and end apart: 2, of which 0 were waited for; matrix products, arithmetic and copies ran while one was open for 7% of the time, Pallas kernels for 0%

profile of v2, /device:TPU:0, one launch (start us, length us, event | category | flops | bytes accessed | tf_op | source)
XLA Modules:
  0.0 211.4 jit_solution(3079401443765181897)
XLA Ops:
  0.0 1.0 copy.19
  1.0 1.0 copy.20
  2.0 0.7 maximum_bitcast_fusion.refs_3_
  2.8 1.9 pad_maximum_fusion.3
  4.7 82.0 %shard_map.118 = (bf16[2048,1024]{1,0:T(8,128)(2,1)}, bf16[2048,1024]{1,0:T(8,128)(2,1)}, bf16[2048,512]{1,0:T(8,128)(2,1)}, bf16[2048,1024]{1,0:T(8,128)(2,1)}, bf16[1024,2048]{1,0:T(8,128)(2,1)}) custom-call(bf16[128,1024]{1,0:T(8,128)(2,1)} %get-tuple-element.33.refs_0_, bf16[128,1024]{1,0:T(8,128)(2,1)} %get-tuple-element.34.refs_1_, ...), custom_call_target="tpu_custom_call" | custom-call | tf_op jit(solution)/shard_map/pallas_call | solution.py:157
  86.8 3.0 %convert_reduce_fusion = f32[1024]{0:T(1024)S(1)} fusion(bf16[1024,2048]{1,0:T(8,128)(2,1)} %get-tuple-element.10), kind=kLoop, calls=%fused_computation.3 | loop fusion | flops 4193280 | bytes 4198400 | tf_op jit(solution)/shard_map/reduce_sum | solution.py:247
  90.2 1.2 fusion.6
  91.5 1.6 fusion.8
  93.6 4.7 %convolution_convert_fusion = bf16[1024,1024]{1,0:T(8,128)(2,1)S(1)} fusion(bf16[1024,2048]{1,0:T(8,128)(2,1)S(1)} %fusion.8, bf16[2048,1024]{1,0:T(8,128)(2,1)S(1)} %copy-done.14), kind=kOutput, calls=%fused_computation.30 | convolution fusion | flops 4296015872 | bytes 10485760 | tf_op jit(solution)/shard_map/dot_general | solution.py:321
  98.4 2.3 %multiply_convert_fusion = bf16[1024,512]{1,0:T(8,128)(2,1)S(1)} fusion(bf16[1024,2048]{1,0:T(8,128)(2,1)S(1)} %fusion.8, bf16[2048,512]{1,0:T(8,128)(2,1)S(1)} %copy-done.15, bf16[1024,1024]{1,0:T(8,128)(2,1)S(1)} %convolution_convert_fusion), kind=kOutput, calls=%fused_computation.29 | convolution fusion | flops 2150105088 | bytes 8388608 | tf_op jit(solution)/shard_map/dot_general | solution.py:324
  100.7 0.6 slice.88
  101.3 3.9 %collective-permute-start.1 = (bf16[2,512]{1,0:T(2,128)(2,1)}, bf16[2,512]{1,0:T(2,128)(2,1)}, u32[]{:S(2)}, u32[]{:S(2)}) collective-permute-start(bf16[2,512]{1,0:T(2,128)(2,1)} %slice.88), channel_id=1, source_target_pairs={{0,8},{8,16},{16,24},{1,9},{9,17},{17,25},{2,10},{10,18},{18,26},{... | collective-permute-start | bytes 6152 | tf_op jit(solution)/shard_map/ppermute | solution.py:242
  105.2 4.8 %convolution_convert_fusion.1 = bf16[1024,1024]{0,1:T(8,128)(2,1)S(1)} fusion(bf16[1024,2048]{1,0:T(8,128)(2,1)S(1)} %fusion.8, bf16[2048,1024]{1,0:T(8,128)(2,1)S(1)} %copy-done.13), kind=kOutput, calls=%fused_computation.31 | convolution fusion | flops 4296015872 | bytes 10485760 | tf_op jit(solution)/shard_map/dot_general | solution.py:320
  110.0 0.8 slice.79
  110.8 3.1 %collective-permute-start = (bf16[128,512]{0,1:T(8,128)(2,1)}, bf16[128,512]{0,1:T(8,128)(2,1)S(1)}, u32[]{:S(2)}, u32[]{:S(2)}) collective-permute-start(bf16[128,512]{0,1:T(8,128)(2,1)} %slice.79), channel_id=1, source_target_pairs={{0,8},{8,16},{16,24},{1,9},{9,17},{17,25},{2,10},{10,18},{18,26},{... | collective-permute-start | bytes 393224 | tf_op jit(solution)/shard_map/ppermute | solution.py:242
  114.0 0.9 fusion.30
  114.9 1.1 fusion.29
  116.0 0.6 fusion.31
  116.8 1.3 fusion.23
  118.1 0.7 max.32
  118.9 1.5 maximum_convert_fusion
  120.5 2.1 %fusion.15 = bf16[1024,512]{1,0:T(8,128)(2,1)S(1)} fusion(f32[1026,512]{1,0:T(8,128)S(1)} %maximum_convert_fusion, bf16[1024,1024]{1,0:T(8,128)(2,1)} %copy-done.5, f32[512]{0:T(512)} %bitcast.81, f32[512]{0:T(512)S(1)} %bitcast.80, f32[512]{0:T(512)S(1)} %bitcast.79), kind=kLoop, calls=%fused_computation.24 | loop fusion | flops 4194304 | bytes 8394752 | tf_op jit(solution)/shard_map/convert_element_type | solution.py:340
  122.8 3.2 %fusion.10 = (f32[4,2,512]{2,1,0:T(2,128)S(1)}, f32[4,640,512,2]{2,1,3,0:T(8,128)S(1)}) fusion(f32[512,640]{0,1:T(8,128)S(1)} %fusion.17, f32[4,2]{1,0:T(4,128)S(1)} %multiply_exponential_fusion, pred[512,640]{0,1:T(8,128)(4,1)S(1)} %copy-done.10, bf16[640,4,64,1]{0,2,3,1:T(8,128)(2,1)S(1)} %bitcast.78, bf16[512,4,2,64]{0,3,2,1:T(8,128)(2,1)S(1)} %bitcast.74), kind=kOutput, calls=%fused_computation.18 | convolution fusion | flops 348647424 | bytes 12992544 | tf_op jit(solution)/shard_map/qkgd,skd->kgqs/dot_general | solution.py:278
  126.0 8.6 %fusion.4 = (f32[4,2,512]{2,1,0:T(2,128)S(1)}, f32[4,2,512]{2,1,0:T(2,128)S(1)}, f32[4,640,512,2]{2,1,3,0:T(8,128)}) fusion(f32[4,640,512,2]{2,1,3,0:T(8,128)S(1)} %get-tuple-element.31, f32[4,2,512]{2,1,0:T(2,128)S(1)} %broadcast_maximum_fusion.1, f32[512,640]{0,1:T(8,128)S(1)} %fusion.17, f32[4,2]{1,0:T(4,128)S(1)} %multiply_exponential_fusion, ...), kind=kOutput, calls=%fused_computation.12 | convolution fusion | flops 361750528 | bytes 23838752 | tf_op jit(solution)/shard_map/qkgd,skd->kgqs/dot_general | solution.py:278
  134.8 4.5 %fusion.22 = bf16[4,64,2,512]{3,1,2,0:T(8,128)(2,1)} fusion(bf16[640,4,64,1]{0,2,3,1:T(8,128)(2,1)S(1)} %bitcast.77, f32[4,640,512,2]{2,1,3,0:T(8,128)S(1)} %get-tuple-element.31, f32[4,2,512]{2,1,0:T(2,128)S(1)} %get-tuple-element.26, f32[4,2,512]{2,1,0:T(2,128)S(1)} %broadcast_maximum_fusion.1, f32[512,640]{0,1:T(8,128)S(1)} %fusion.17, ...), kind=kOutput, calls=%fused_computation.39 | convolution fusion | flops 354156544 | bytes 13008928 | tf_op jit(solution)/shard_map/kgqs,skd->qkgd/dot_general | solution.py:289
  139.3 1.3 copy.23
  140.6 7.0 %fusion.5 = f32[4,2,512]{2,1,0:T(2,128)S(1)} fusion(f32[4,640,512,2]{2,1,3,0:T(8,128)} %get-tuple-element.32, f32[4,2,512]{2,1,0:T(2,128)S(1)} %get-tuple-element.27, f32[512,640]{0,1:T(8,128)S(1)} %fusion.17, f32[4,2]{1,0:T(4,128)S(1)} %multiply_exponential_fusion, pred[512,640]{0,1:T(8,128)(4,1)S(1)} %copy-done.3), kind=kLoop, calls=%fused_computation.13 | loop fusion | flops 15724544 | bytes 12156960 | tf_op jit(solution)/shard_map/reduce_sum | solution.py:287
  147.7 4.5 %fusion.21 = bf16[4,64,2,512]{3,1,2,0:T(8,128)(2,1)} fusion(bf16[640,4,64,1]{0,2,3,1:T(8,128)(2,1)S(1)} %bitcast.75, f32[4,640,512,2]{2,1,3,0:T(8,128)S(1)} %copy-done.1, f32[4,2,512]{2,1,0:T(2,128)S(1)} %exponential_add_fusion, f32[4,2,512]{2,1,0:T(2,128)S(1)} %get-tuple-element.27, f32[512,640]{0,1:T(8,128)S(1)} %fusion.17, ...), kind=kOutput, calls=%fused_computation.38 | convolution fusion | flops 354156544 | bytes 13008928 | tf_op jit(solution)/shard_map/kgqs,skd->qkgd/dot_general | solution.py:289
  152.2 1.3 copy.24
  153.4 1.6 pad_maximum_fusion.mix
  155.1 53.2 %shard_map.119 = bf16[512,2048]{1,0:T(8,128)(2,1)} custom-call(bf16[1024,1024]{1,0:T(8,128)(2,1)} %pad_maximum_fusion.mix, bf16[2048,1024]{1,0:T(8,128)(2,1)} %get-tuple-element.14.w_out), custom_call_target="tpu_custom_call" | custom-call | tf_op jit(solution)/shard_map/pallas_call | solution.py:224
  208.3 3.2 %copy.32 = bf16[1,512,2048]{2,1,0:T(8,128)(2,1)} copy(bf16[1,512,2048]{2,1,0:T(8,128)(2,1)} %bitcast.69) | data formatting | bytes 4194304
  (46 shorter events, 1.6 us)
Async XLA Ops:
  86.8 3.5 %copy-start = (bf16[1024,2048]{1,0:T(8,128)(2,1)S(1)}, bf16[1024,2048]{1,0:T(8,128)(2,1)}, u32[]{:S(2)}) copy-start(bf16[1024,2048]{1,0:T(8,128)(2,1)} %get-tuple-element.10) | copy-start | bytes 12582916
  86.8 4.7 %copy-start.12 = (f32[2048]{0:T(1024)S(1)}, f32[2048]{0:T(1024)}, u32[]{:S(2)}) copy-start(f32[2048]{0:T(1024)} %param.13) | copy-start | bytes 24580
  91.5 2.2 %copy-start.14 = (bf16[2048,1024]{1,0:T(8,128)(2,1)S(1)}, bf16[2048,1024]{1,0:T(8,128)(2,1)}, u32[]{:S(2)}) copy-start(bf16[2048,1024]{1,0:T(8,128)(2,1)} %get-tuple-element.12) | copy-start | bytes 12582916
  93.6 4.7 %copy-start.15 = (bf16[2048,512]{1,0:T(8,128)(2,1)S(1)}, bf16[2048,512]{1,0:T(8,128)(2,1)}, u32[]{:S(2)}) copy-start(bf16[2048,512]{1,0:T(8,128)(2,1)} %get-tuple-element.13) | copy-start | bytes 6291460
  98.3 2.4 %copy-start.5 = (bf16[1024,1024]{1,0:T(8,128)(2,1)}, bf16[1024,1024]{1,0:T(8,128)(2,1)S(1)}, u32[]{:S(2)}) copy-start(bf16[1024,1024]{1,0:T(8,128)(2,1)S(1)} %convolution_convert_fusion) | copy-start | bytes 6291460
  98.4 6.8 %copy-start.13 = (bf16[2048,1024]{1,0:T(8,128)(2,1)S(1)}, bf16[2048,1024]{1,0:T(8,128)(2,1)}, u32[]{:S(2)}) copy-start(bf16[2048,1024]{1,0:T(8,128)(2,1)} %get-tuple-element.11) | copy-start | bytes 12582916
  100.7 4.5 %copy-start.4 = (bf16[1024,512]{1,0:T(8,128)(2,1)}, bf16[1024,512]{1,0:T(8,128)(2,1)S(1)}, u32[]{:S(2)}) copy-start(bf16[1024,512]{1,0:T(8,128)(2,1)S(1)} %multiply_convert_fusion) | copy-start | bytes 3145732
  101.3 17.5 %collective-permute-start.1 = (bf16[2,512]{1,0:T(2,128)(2,1)}, bf16[2,512]{1,0:T(2,128)(2,1)}, u32[]{:S(2)}, u32[]{:S(2)}) collective-permute-start(bf16[2,512]{1,0:T(2,128)(2,1)} %slice.88), channel_id=1, source_target_pairs={{0,8},{8,16},{16,24},{1,9},{9,17},{17,25},{2,10},{10,18},{18,26},{... | collective-permute-start | bytes 6152 | tf_op jit(solution)/shard_map/ppermute | solution.py:242
  105.2 10.8 %copy-start.11 = (bf16[3,512]{1,0:T(4,128)(2,1)S(1)}, bf16[3,512]{1,0:T(4,128)(2,1)}, u32[]{:S(2)}) copy-start(bf16[3,512]{1,0:T(4,128)(2,1)} %param.20) | copy-start | bytes 9220
  110.0 10.4 %copy-start.2 = (bf16[1024,1024]{0,1:T(8,128)(2,1)}, bf16[1024,1024]{0,1:T(8,128)(2,1)S(1)}, u32[]{:S(2)}) copy-start(bf16[1024,1024]{0,1:T(8,128)(2,1)S(1)} %convolution_convert_fusion.1) | copy-start | bytes 6291460
  110.8 11.8 %collective-permute-start = (bf16[128,512]{0,1:T(8,128)(2,1)}, bf16[128,512]{0,1:T(8,128)(2,1)S(1)}, u32[]{:S(2)}, u32[]{:S(2)}) collective-permute-start(bf16[128,512]{0,1:T(8,128)(2,1)} %slice.79), channel_id=1, source_target_pairs={{0,8},{8,16},{16,24},{1,9},{9,17},{17,25},{2,10},{10,18},{18,26},{... | collective-permute-start | bytes 393224 | tf_op jit(solution)/shard_map/ppermute | solution.py:242
  120.4 2.2 %slice-start = ((bf16[1024,1024]{0,1:T(8,128)(2,1)}), bf16[1024,512]{0,1:T(8,128)(2,1)S(1)}, s32[]{:S(2)}) async-start(bf16[1024,1024]{0,1:T(8,128)(2,1)} %copy-done.2), calls=%async_computation | async-start | bytes 2097152 | tf_op jit(solution)/shard_map/slice | solution.py:322
  120.4 2.3 %copy-start.7 = (bf16[512,512]{0,1:T(8,128)(2,1)S(1)}, bf16[512,512]{0,1:T(8,128)(2,1)}, u32[]{:S(2)}) copy-start(bf16[512,512]{0,1:T(8,128)(2,1)} %get-tuple-element.17) | copy-start | bytes 1572868
  120.4 2.3 %copy-start.10 = (pred[512,640]{0,1:T(8,128)(4,1)S(1)}, pred[512,640]{0,1:T(8,128)(4,1)}, u32[]{:S(2)}) copy-start(pred[512,640]{0,1:T(8,128)(4,1)} %get-tuple-element.29) | copy-start | bytes 983044
  122.7 3.3 %copy-start.3 = (pred[512,640]{0,1:T(8,128)(4,1)S(1)}, pred[512,640]{0,1:T(8,128)(4,1)}, u32[]{:S(2)}) copy-start(pred[512,640]{0,1:T(8,128)(4,1)} %get-tuple-element.28) | copy-start | bytes 983044
  122.7 3.3 %copy-start.6 = (bf16[512,512]{0,1:T(8,128)(2,1)S(1)}, bf16[512,512]{0,1:T(8,128)(2,1)}, u32[]{:S(2)}) copy-start(bf16[512,512]{0,1:T(8,128)(2,1)} %get-tuple-element.18) | copy-start | bytes 1572868
  122.7 3.3 %copy-start.9 = (bf16[640,256]{0,1:T(8,128)(2,1)S(1)}, bf16[640,256]{0,1:T(8,128)(2,1)}, u32[]{:S(2)}) copy-start(bf16[640,256]{0,1:T(8,128)(2,1)} %get-tuple-element.19) | copy-start | bytes 983044
  140.6 7.1 %copy-start.1 = (f32[4,640,512,2]{2,1,3,0:T(8,128)S(1)}, f32[4,640,512,2]{2,1,3,0:T(8,128)}, u32[]{:S(2)}) copy-start(f32[4,640,512,2]{2,1,3,0:T(8,128)} %get-tuple-element.32) | copy-start | bytes 31457284
  140.6 7.1 %copy-start.8 = (bf16[640,256]{0,1:T(8,128)(2,1)S(1)}, bf16[640,256]{0,1:T(8,128)(2,1)}, u32[]{:S(2)}) copy-start(bf16[640,256]{0,1:T(8,128)(2,1)} %get-tuple-element.20) | copy-start | bytes 983044
